TPU v7x, 512 devices: a 4x2x32 block of a 4x8x32 slice. The times are simulated.
512 devices in a mesh: grp: 2 (over y), kv: 32 (over z), tp: 8 (over x, core).
Axes of the slice: x: 4, y: 2, z: 32, core: 2. Of those that a mesh axis runs over, the one named last changes fastest.
The devices are a block of a 4x8x32 slice.
Arguments:
- tokens: bfloat16 [256, 2048], P('grp', ('kv', 'tp')), parts along dimension 0, may hold values from -13 to 13, as said below
- state: float32 [256, 16, 128, 128], P(('grp', 'kv'), 'tp'), parts along dimension 0, may hold values from -0.6 to 0.6
- norm_gain: bfloat16 [2048], P('kv'), may hold values from 0.099609375 to 1.8984375
- w_query: bfloat16 [2048, 2048], P('kv', 'tp'), may hold values from -0.125 to 0.125
- w_key: bfloat16 [2048, 2048], P('kv', 'tp'), may hold values from -0.125 to 0.125
- w_value: bfloat16 [2048, 2048], P('kv', 'tp'), may hold values from -0.125 to 0.125
- w_beta: bfloat16 [2048, 16], replicated, may hold values from -0.125 to 0.125
- w_decay: bfloat16 [2048, 16], replicated, may hold values from -0.125 to 0.125
- a_log: float32 [16], P('tp'), may hold values from -3 to 1
- dt_bias: float32 [16], P('tp'), may hold values from -2 to 1
- head_gain: float32 [128], replicated, may hold values from 0.1 to 1.9
- w_out: bfloat16 [2048, 2048], P('tp', 'kv'), may hold values from -0.125 to 0.125
- mixer_gain: bfloat16 [2048], P('kv'), may hold values from 0.099609375 to 1.8984375
- w_up: bfloat16 [2048, 8192], P('kv', 'tp'), may hold values from -0.125 to 0.125
- w_down: bfloat16 [8192, 2048], P('tp', 'kv'), may hold values from -0.0625 to 0.0625
Outputs:
- mixed: bfloat16 [256, 2048], P('grp', ('kv', 'tp')), parts along dimension 0
- new_state: float32 [256, 16, 128, 128], P(('grp', 'kv'), 'tp'), parts along dimension 0
There are 2 independent parts, one for each index of `grp`. A program takes and returns all parts, laid end to end along the dimension named above; an argument that names none is the same for every part. Nothing has to cross between parts.
Inputs may be any that keep to these rules, and one draw needn't show every extreme that they name: `tokens`: activations of order one.
All inputs are finite; a program needn't handle non-finite values.
Results may differ from a plain program's by a relative error of at most 0.019.
Values may be sent and summed in bfloat16 or wider, within the bound.
No kernel may reach another device: no remote copies, remote signals or barrier semaphores. Data moves between devices by JAX's collectives and lax.ppermute only.
A program may use at most 64 MiB of HBM per device.

v0:
```python
import jax
import jax.numpy as jnp
from jax import lax
from jax.sharding import Mesh
from jax.sharding import PartitionSpec as P


epsilon = 1e-06
bf16 = jnp.bfloat16
f32 = jnp.float32
KV = ("hi", "mid", "pair")
LO = ("mid", "pair")
NEIGHBOURS = 8


def exchange(x, axis):
    return lax.all_to_all(x, axis, split_axis=0, concat_axis=0, tiled=True)


def from_everyone(x, axis):
    return exchange(jnp.broadcast_to(x, (lax.axis_size(axis), *x.shape)), axis)


def dotted(left, right, left_dim, right_dim):
    dims = (((left_dim,), (right_dim,)), ((), ()))
    return lax.dot_general(left, right, dims, preferred_element_type=f32)


def delta_update(
    query_pre, key_pre, value_pre, beta_pre, decay_pre, state, a_log, dt_bias, head_gain
):
    query = query_pre * lax.rsqrt(jnp.sum(query_pre * query_pre, axis=-1, keepdims=True) + epsilon)
    keyed = key_pre * lax.rsqrt(jnp.sum(key_pre * key_pre, axis=-1, keepdims=True) + epsilon)
    beta = jax.nn.sigmoid(beta_pre)
    decay = jnp.exp(-jnp.exp(a_log) * jax.nn.softplus(decay_pre + dt_bias))
    key_read = jnp.einsum("bhk,bhkv->bhv", keyed, state)
    query_read = jnp.einsum("bhk,bhkv->bhv", query, state)
    fresh = beta[..., None] * (value_pre - decay[..., None] * key_read)
    new_state = decay[..., None, None] * state + keyed[..., :, None] * fresh[..., None, :]
    intersection = jnp.sum(query * keyed, axis=-1)
    reading = decay[..., None] * query_read + intersection[..., None] * fresh
    normed = (
        reading
        * lax.rsqrt(jnp.mean(reading * reading, axis=-1, keepdims=True) + epsilon)
        * head_gain
    )
    return (normed.astype(bf16), new_state)


def mixer_weights(w_up, w_down, mixer_gain, n_tp):
    near = lax.axis_size(LO)
    me = lax.axis_index(LO)
    block, wide = w_up.shape
    share = wide // near
    gained = (w_up.astype(f32) * mixer_gain.astype(f32)[:, None]).astype(bf16)
    both = jnp.concatenate([gained, w_down.T], axis=0)
    both = both.reshape(2 * block, near, share).transpose(1, 0, 2)
    whole = jnp.zeros_like(both)
    for step in range(near):
        piece = lax.dynamic_slice_in_dim(both, me ^ step, 1, axis=0)
        if step:
            piece = lax.ppermute(piece, LO, [(i, i ^ step) for i in range(near)])
        whole = lax.dynamic_update_slice_in_dim(whole, piece, me ^ step, axis=0)
    up = whole[:, :block].reshape(near * block, share)
    down_t = whole[:, block:].reshape(near, n_tp, block // n_tp, share)
    down_t = down_t.transpose(1, 0, 2, 3).reshape(near * block, share)
    return up, down_t


def local(
    tokens,
    state,
    norm_gain,
    w_query,
    w_key,
    w_value,
    w_beta,
    w_decay,
    a_log,
    dt_bias,
    head_gain,
    w_out,
    mixer_gain,
    w_up,
    w_down,
):
    seq_here, heads_here, head_size = state.shape[:3]
    n_kv = lax.axis_size(KV)
    n_tp = lax.axis_size("tp")
    n_near = lax.axis_size(LO)
    width = w_beta.shape[0]
    rows, own = tokens.shape
    block = own * n_tp
    kv_index = lax.axis_index(KV)
    tp_index = lax.axis_index("tp")
    side = lax.axis_index("pair")
    columns = heads_here * head_size
    assert heads_here == lax.axis_size("pair")

    tokens_t = tokens.T
    gain = norm_gain.astype(f32)[:, None]
    split = lambda w: w.reshape(block, heads_here, head_size).transpose(1, 0, 2)
    by_head = jnp.concatenate([split(w_query), split(w_key), split(w_value)], axis=2)
    by_head = (by_head.astype(f32) * gain).astype(bf16)
    kept = lax.dynamic_index_in_dim(by_head, side, 0, keepdims=False)
    given = lax.dynamic_index_in_dim(by_head, 1 - side, 0, keepdims=False)
    taken = lax.ppermute(given, "pair", [(0, 1), (1, 0)])

    both = from_everyone(tokens_t, ("pair", "tp")).reshape(2, block, rows)
    mine = lax.dynamic_index_in_dim(both, side, 0, keepdims=False)
    other = lax.dynamic_index_in_dim(both, 1 - side, 0, keepdims=False)
    inputs = mine.astype(f32)
    scaled = (inputs * gain).astype(bf16)
    squares = jnp.sum(inputs * inputs, axis=0)
    at = (kv_index * block, tp_index * heads_here)
    beta_rows = lax.dynamic_slice(w_beta, at, (block, heads_here))
    decay_rows = lax.dynamic_slice(w_decay, at, (block, heads_here))
    parts = [
        (dotted(mine, kept, 0, 0) + dotted(other, taken, 0, 0)).astype(bf16),
        dotted(scaled, jnp.concatenate([beta_rows, decay_rows], axis=1), 0, 0).astype(bf16),
        squares[:, None].astype(bf16),
    ]
    sent = jnp.concatenate(parts, axis=1).reshape(n_kv, seq_here, -1)
    arrived = exchange(sent, KV)
    main = 3 * head_size
    sums = arrived.astype(f32)
    gates = sums[..., main:].sum(axis=0)
    sums = sums[..., :main].reshape(-1, heads_here, seq_here, main).sum(axis=0)
    first = lax.rsqrt(gates[:, -1:] / width + epsilon)
    pre = (first * sums).transpose(1, 0, 2)
    gates = first * gates
    heads = lambda n: pre[..., n * head_size : (n + 1) * head_size]
    normed, new_state = delta_update(
        heads(0),
        heads(1),
        heads(2),
        gates[:, :heads_here],
        gates[:, heads_here : 2 * heads_here],
        state,
        a_log,
        dt_bias,
        head_gain,
    )
    up, down_t = mixer_weights(w_up, w_down, mixer_gain, n_tp)

    every = from_everyone(normed.reshape(seq_here, columns), KV).reshape(rows, columns)
    every, up, down_t, new_state = lax.optimization_barrier((every, up, down_t, new_state))
    head_part = dotted(w_out, every, 0, 1).astype(bf16)
    attended = from_everyone(head_part, "tp").astype(f32).sum(axis=0)
    middle_block = (inputs + attended).astype(bf16)
    middle_own = lax.dynamic_slice_in_dim(middle_block, tp_index * own, own, axis=0)

    middle = from_everyone(middle_block, LO).reshape(n_near * block, rows)
    middle_f = middle.astype(f32)
    squares_two = jnp.sum(middle_f * middle_f, axis=0, keepdims=True)
    hidden_part = dotted(up, middle, 0, 0)
    tail = jnp.broadcast_to(squares_two, (8, rows))
    sent = jnp.concatenate([hidden_part, tail], axis=0).astype(bf16)
    sums = from_everyone(sent, "hi").astype(f32).sum(axis=0)
    second = lax.rsqrt(sums[-1:] / width + epsilon)
    hidden = jnp.square(jax.nn.relu(second * sums[:-8])).astype(bf16)
    down_part = dotted(down_t, hidden, 1, 0).astype(bf16)
    arrived = exchange(down_part.reshape(n_tp, n_near * own, rows), "tp")
    near_part = arrived.astype(f32).sum(axis=0).astype(bf16)
    arrived = exchange(near_part.reshape(n_near, own, rows), LO)
    lowered = arrived.astype(f32).sum(axis=0)
    mixed = (middle_own.astype(f32) + lowered).astype(bf16).T
    return (mixed, new_state)


def solution(mesh):
    near = min(NEIGHBOURS, mesh.shape["kv"])
    devices = mesh.devices.reshape(mesh.shape["grp"], -1, near // 2, 2, mesh.shape["tp"])
    fine = Mesh(devices, ("grp", *KV, "tp"))
    every = (*KV, "tp")
    return jax.shard_map(
        local,
        mesh=fine,
        in_specs=(
            P("grp", every),
            P(("grp", *KV), "tp", None, None),
            P(KV),
            P(KV, "tp"),
            P(KV, "tp"),
            P(KV, "tp"),
            P(),
            P(),
            P("tp"),
            P("tp"),
            P(),
            P("tp", KV),
            P(KV),
            P(KV, "tp"),
            P("tp", KV),
        ),
        out_specs=(P("grp", every), P(("grp", *KV), "tp", None, None)),
        check_vma=False,
    )
```

profile of v0, /device:TPU:33, one launch (start us, length us, event | category | flops | bytes accessed | tf_op | source)
XLA Modules:
  0.0 237.5 jit_solution(3880891686193219358)
XLA Ops:
  0.6 1.3 broadcast_in_dim.14
  2.0 44.9 %all-to-all-start = ((bf16[16,8,128]{2,1,0:T(8,128)(2,1)}), bf16[16,8,128]{2,1,0:T(8,128)(2,1)S(1)}, u32[]{:S(2)}, u32[]{:S(2)}) async-start(bf16[16,8,128]{2,1,0:T(8,128)(2,1)} %broadcast_in_dim.14), calls=%async_computation | async-start | bytes 65536 | tf_op jit(solution)/shard_map/all_to_all | solution.py:17
  46.8 0.6 copy-done.9
  47.5 0.7 copy-done.5
  48.3 0.7 copy-done.6
  49.0 0.1 multiply_convert_fusion.1
  49.2 0.2 constant_dynamic-slice_fusion.9
  49.4 3.6 %collective-permute-start = (bf16[64,384]{1,0:T(8,128)(2,1)S(1)}, bf16[64,384]{1,0:T(8,128)(2,1)S(1)}, u32[]{:S(2)}, u32[]{:S(2)}) collective-permute-start(bf16[64,384]{1,0:T(8,128)(2,1)S(1)} %bitcast.91), channel_id=1, source_target_pairs={{0,8},{8,0},{1,9},{9,1},{2,10},{10,2},{3,11},{11,3},{4,12},{12,4},... | collective-permute-start | bytes 147464 | tf_op jit(solution)/shard_map/ppermute | solution.py:107
  53.0 0.6 copy-done.10
  53.7 0.1 multiply_convert_fusion
  53.8 0.8 copy-done.3
  54.6 0.2 copy.98
  54.9 0.1 copy.100
  55.0 2.0 collective-permute-start.1
  56.9 0.1 copy.101
  57.1 2.0 collective-permute-start.2
  59.0 0.1 copy.102
  59.1 5.5 %collective-permute-start.3 = (bf16[1,128,128]{2,1,0:T(8,128)(2,1)S(1)}, bf16[1,128,128]{2,1,0:T(8,128)(2,1)S(1)}, u32[]{:S(2)}, u32[]{:S(2)}) collective-permute-start(bf16[1,128,128]{2,1,0:T(8,128)(2,1)S(1)} %bitcast.93), channel_id=1, source_target_pairs={{0,24},{8,16},{16,8},{24,0},{32,56},{40,48},{48,40},{56,32},{1,25}... | collective-permute-start | bytes 98312 | tf_op jit(solution)/shard_map/ppermute | solution.py:62
  64.6 0.1 copy.103
  64.7 2.0 collective-permute-start.4
  66.7 0.8 dynamic_slice.51
  67.5 0.8 dynamic_slice.52
  68.2 0.1 copy.104
  68.3 0.1 copy.99
  68.5 0.2 fusion.8
  68.8 0.2 convolution_convert_fusion.3
  68.9 0.1 copy.114
  69.1 0.2 convert_element_type.113
  69.4 6.1 %collective-permute-start.5 = (bf16[1,128,128]{2,1,0:T(8,128)(2,1)S(1)}, bf16[1,128,128]{2,1,0:T(8,128)(2,1)S(1)}, u32[]{:S(2)}, u32[]{:S(2)}) collective-permute-start(bf16[1,128,128]{2,1,0:T(8,128)(2,1)S(1)} %bitcast.97), channel_id=1, source_target_pairs={{0,40},{8,32},{16,56},{24,48},{32,8},{40,0},{48,24},{56,16},{1,41}... | collective-permute-start | bytes 98312 | tf_op jit(solution)/shard_map/ppermute | solution.py:62
  75.5 0.2 fusion.1
  75.8 0.7 pad_maximum_fusion.1
  76.5 8.5 %all-to-all-start.1 = ((bf16[32,4,389]{2,1,0:T(4,128)(2,1)}), bf16[32,4,389]{2,1,0:T(4,128)(2,1)S(1)}, u32[]{:S(2)}, u32[]{:S(2)}) async-start(bf16[32,4,389]{2,1,0:T(4,128)(2,1)} %pad_maximum_fusion.1), calls=%async_computation.1 | async-start | bytes 262144 | tf_op jit(solution)/shard_map/all_to_all | solution.py:17
  85.1 0.1 copy.106
  85.2 0.1 copy.105
  85.3 8.4 %collective-permute-start.6 = (bf16[1,128,128]{2,1,0:T(8,128)(2,1)S(1)}, bf16[1,128,128]{2,1,0:T(8,128)(2,1)S(1)}, u32[]{:S(2)}, u32[]{:S(2)}) collective-permute-start(bf16[1,128,128]{2,1,0:T(8,128)(2,1)S(1)} %bitcast.98), channel_id=1, source_target_pairs={{0,48},{8,56},{16,32},{24,40},{32,16},{40,24},{48,0},{56,8},{1,49}... | collective-permute-start | bytes 98312 | tf_op jit(solution)/shard_map/ppermute | solution.py:62
  93.8 3.1 %collective-permute-start.7 = (bf16[1,128,128]{2,1,0:T(8,128)(2,1)S(1)}, bf16[1,128,128]{2,1,0:T(8,128)(2,1)S(1)}, u32[]{:S(2)}, u32[]{:S(2)}) collective-permute-start(bf16[1,128,128]{2,1,0:T(8,128)(2,1)S(1)} %bitcast.94), channel_id=1, source_target_pairs={{0,56},{8,48},{16,40},{24,32},{32,24},{40,16},{48,8},{56,0},{1,57}... | collective-permute-start | bytes 98312 | tf_op jit(solution)/shard_map/ppermute | solution.py:62
  97.0 6.0 %collective-permute-done.6 = bf16[1,128,128]{2,1,0:T(8,128)(2,1)S(1)} collective-permute-done((bf16[1,128,128]{2,1,0:T(8,128)(2,1)S(1)}, bf16[1,128,128]{2,1,0:T(8,128)(2,1)S(1)}, u32[]{:S(2)}, u32[]{:S(2)}) %collective-permute-start.6) | collective-permute-done | bytes 32800 | tf_op jit(solution)/shard_map/ppermute | solution.py:62
  103.1 9.6 %all-to-all-done.1 = bf16[32,4,389]{2,1,0:T(4,128)(2,1)S(1)} async-done(((bf16[32,4,389]{2,1,0:T(4,128)(2,1)}), bf16[32,4,389]{2,1,0:T(4,128)(2,1)S(1)}, u32[]{:S(2)}, u32[]{:S(2)}) %all-to-all-start.1) | async-done | bytes 99616 | tf_op jit(solution)/shard_map/all_to_all | solution.py:17
  112.7 0.2 rsqrt_reduce_fusion
  113.1 0.1 multiply_reduce_fusion.3
  113.4 0.6 copy-done.7
  113.9 0.1 fusion.38
  114.0 0.1 copy.97
  114.1 0.1 copy.96
  114.3 0.2 fusion.31
  114.5 0.2 fusion.29
  114.7 0.2 multiply_reduce_fusion.1
  115.0 0.7 copy-done.8
  115.7 0.6 broadcast_in_dim.15
  116.4 9.0 %all-to-all-start.2 = ((bf16[32,4,256]{2,1,0:T(4,128)(2,1)}), bf16[32,4,256]{2,1,0:T(4,128)(2,1)S(1)}, u32[]{:S(2)}, u32[]{:S(2)}) async-start(bf16[32,4,256]{2,1,0:T(4,128)(2,1)} %broadcast_in_dim.15), calls=%async_computation.2 | async-start | bytes 131072 | tf_op jit(solution)/shard_map/all_to_all | solution.py:17
  125.5 1.0 multiply_add_fusion
  126.6 21.6 %all-to-all-done.2 = bf16[32,4,256]{2,1,0:T(4,128)(2,1)S(1)} async-done(((bf16[32,4,256]{2,1,0:T(4,128)(2,1)}), bf16[32,4,256]{2,1,0:T(4,128)(2,1)S(1)}, u32[]{:S(2)}, u32[]{:S(2)}) %all-to-all-start.2) | async-done | bytes 65568 | tf_op jit(solution)/shard_map/all_to_all | solution.py:17
  148.2 0.1 fusion.2
  148.4 12.8 %all_to_all.40 = bf16[8,64,128]{2,1,0:T(8,128)(2,1)S(1)} all-to-all(bf16[8,64,128]{2,1,0:T(8,128)(2,1)S(1)} %broadcast_in_dim.17), channel_id=1, replica_groups=mesh['grp'=2,'hi'=4,'mid'=4,'pair'=2,'tp'=8] {'tp'}, dimensions={0} | all-to-all | bytes 262144 | tf_op jit(solution)/shard_map/all_to_all | solution.py:17
  161.2 12.8 %all_to_all.41 = bf16[8,64,128]{2,1,0:T(8,128)(2,1)S(1)} all-to-all(bf16[8,64,128]{2,1,0:T(8,128)(2,1)S(1)} %broadcast_in_dim.18), channel_id=1, replica_groups=mesh['grp'=2,'hi'=4,'mid'=4,'pair'=2,'tp'=8] {'mid','pair'}, dimensions={0} | all-to-all | bytes 262144 | tf_op jit(solution)/shard_map/all_to_all | solution.py:17
  174.1 0.2 convolution_convert_fusion.1
  174.3 0.1 multiply_reduce_fusion
  174.5 29.2 %all_to_all.42 = bf16[4,136,128]{2,1,0:T(8,128)(2,1)S(1)} all-to-all(bf16[4,136,128]{2,1,0:T(8,128)(2,1)S(1)} %broadcast_in_dim.20), channel_id=1, replica_groups=mesh['grp'=2,'hi'=4,'mid'=4,'pair'=2,'tp'=8] {'hi'}, dimensions={0} | all-to-all | bytes 278528 | tf_op jit(solution)/shard_map/all_to_all | solution.py:17
  203.7 0.2 convolution_convert_fusion
  203.9 15.1 %all_to_all.43 = bf16[8,64,128]{2,1,0:T(8,128)(2,1)S(1)} all-to-all(bf16[8,64,128]{2,1,0:T(8,128)(2,1)S(1)} %bitcast.79), channel_id=1, replica_groups=mesh['grp'=2,'hi'=4,'mid'=4,'pair'=2,'tp'=8] {'tp'}, dimensions={0} | all-to-all | bytes 262144 | tf_op jit(solution)/shard_map/all_to_all | solution.py:17
  219.0 0.6 reduce_sum.121
  219.6 7.9 %all-to-all-start.7 = ((bf16[8,8,128]{2,1,0:T(8,128)(2,1)}), bf16[8,8,128]{2,1,0:T(8,128)(2,1)S(1)}, u32[]{:S(2)}, u32[]{:S(2)}) async-start(bf16[8,8,128]{2,1,0:T(8,128)(2,1)} %bitcast.33), calls=%async_computation.7 | async-start | bytes 32768 | tf_op jit(solution)/shard_map/all_to_all | solution.py:17
  227.6 9.4 %all-to-all-done.7 = bf16[8,8,128]{2,1,0:T(8,128)(2,1)S(1)} async-done(((bf16[8,8,128]{2,1,0:T(8,128)(2,1)}), bf16[8,8,128]{2,1,0:T(8,128)(2,1)S(1)}, u32[]{:S(2)}, u32[]{:S(2)}) %all-to-all-start.7) | async-done | bytes 16416 | tf_op jit(solution)/shard_map/all_to_all | solution.py:17
  236.9 0.6 fusion.36
  (73 shorter events, 1.3 us)
Async XLA Ops:
  0.6 147.6 %copy-start = (bf16[256,64]{0,1:T(8,128)(2,1)S(1)}, bf16[256,64]{0,1:T(8,128)(2,1)}, u32[]{:S(2)}) copy-start(bf16[256,64]{0,1:T(8,128)(2,1)} %param.26) | copy-start | bytes 98308
  2.0 45.5 %copy-start.4 = (bf16[64,256]{1,0:T(8,128)(2,1)S(1)}, bf16[64,256]{1,0:T(8,128)(2,1)}, u32[]{:S(2)}) copy-start(bf16[64,256]{1,0:T(8,128)(2,1)} %param.18) | copy-start | bytes 98308
  2.0 66.6 %all-to-all-start = ((bf16[16,8,128]{2,1,0:T(8,128)(2,1)}), bf16[16,8,128]{2,1,0:T(8,128)(2,1)S(1)}, u32[]{:S(2)}, u32[]{:S(2)}) async-start(bf16[16,8,128]{2,1,0:T(8,128)(2,1)} %broadcast_in_dim.14), calls=%async_computation | async-start | bytes 65536 | tf_op jit(solution)/shard_map/all_to_all | solution.py:17
  46.8 0.7 copy-start.9
  47.5 0.8 copy-start.5
  48.2 0.8 copy-start.6
  49.4 4.3 %copy-start.2 = (bf16[64,1024]{1,0:T(8,128)(2,1)S(1)}, bf16[64,1024]{1,0:T(8,128)(2,1)}, u32[]{:S(2)}) copy-start(bf16[64,1024]{1,0:T(8,128)(2,1)} %param.28) | copy-start | bytes 393220
  49.4 20.0 %collective-permute-start = (bf16[64,384]{1,0:T(8,128)(2,1)S(1)}, bf16[64,384]{1,0:T(8,128)(2,1)S(1)}, u32[]{:S(2)}, u32[]{:S(2)}) collective-permute-start(bf16[64,384]{1,0:T(8,128)(2,1)S(1)} %bitcast.91), channel_id=1, source_target_pairs={{0,8},{8,0},{1,9},{9,1},{2,10},{10,2},{3,11},{11,3},{4,12},{12,4},... | collective-permute-start | bytes 147464 | tf_op jit(solution)/shard_map/ppermute | solution.py:107
  53.0 0.7 copy-start.10
  53.7 0.9 copy-start.3
  55.0 30.4 %collective-permute-start.1 = (bf16[1,128,128]{2,1,0:T(8,128)(2,1)S(1)}, bf16[1,128,128]{2,1,0:T(8,128)(2,1)S(1)}, u32[]{:S(2)}, u32[]{:S(2)}) collective-permute-start(bf16[1,128,128]{2,1,0:T(8,128)(2,1)S(1)} %bitcast.96), channel_id=1, source_target_pairs={{0,8},{8,0},{16,24},{24,16},{32,40},{40,32},{48,56},{56,48},{1,9},... | collective-permute-start | bytes 98312 | tf_op jit(solution)/shard_map/ppermute | solution.py:62
  57.1 36.7 %collective-permute-start.2 = (bf16[1,128,128]{2,1,0:T(8,128)(2,1)S(1)}, bf16[1,128,128]{2,1,0:T(8,128)(2,1)S(1)}, u32[]{:S(2)}, u32[]{:S(2)}) collective-permute-start(bf16[1,128,128]{2,1,0:T(8,128)(2,1)S(1)} %bitcast.95), channel_id=1, source_target_pairs={{0,16},{8,24},{16,0},{24,8},{32,48},{40,56},{48,32},{56,40},{1,17}... | collective-permute-start | bytes 98312 | tf_op jit(solution)/shard_map/ppermute | solution.py:62
  59.1 37.8 %collective-permute-start.3 = (bf16[1,128,128]{2,1,0:T(8,128)(2,1)S(1)}, bf16[1,128,128]{2,1,0:T(8,128)(2,1)S(1)}, u32[]{:S(2)}, u32[]{:S(2)}) collective-permute-start(bf16[1,128,128]{2,1,0:T(8,128)(2,1)S(1)} %bitcast.93), channel_id=1, source_target_pairs={{0,24},{8,16},{16,8},{24,0},{32,56},{40,48},{48,40},{56,32},{1,25}... | collective-permute-start | bytes 98312 | tf_op jit(solution)/shard_map/ppermute | solution.py:62
  64.7 32.3 %collective-permute-start.4 = (bf16[1,128,128]{2,1,0:T(8,128)(2,1)S(1)}, bf16[1,128,128]{2,1,0:T(8,128)(2,1)S(1)}, u32[]{:S(2)}, u32[]{:S(2)}) collective-permute-start(bf16[1,128,128]{2,1,0:T(8,128)(2,1)S(1)} %bitcast.92), channel_id=1, source_target_pairs={{0,32},{8,40},{16,48},{24,56},{32,0},{40,8},{48,16},{56,24},{1,33}... | collective-permute-start | bytes 98312 | tf_op jit(solution)/shard_map/ppermute | solution.py:62
  69.4 27.6 %collective-permute-start.5 = (bf16[1,128,128]{2,1,0:T(8,128)(2,1)S(1)}, bf16[1,128,128]{2,1,0:T(8,128)(2,1)S(1)}, u32[]{:S(2)}, u32[]{:S(2)}) collective-permute-start(bf16[1,128,128]{2,1,0:T(8,128)(2,1)S(1)} %bitcast.97), channel_id=1, source_target_pairs={{0,40},{8,32},{16,56},{24,48},{32,8},{40,0},{48,24},{56,16},{1,41}... | collective-permute-start | bytes 98312 | tf_op jit(solution)/shard_map/ppermute | solution.py:62
  76.5 8.6 %copy-start.11 = (f32[2]{0:T(128)S(1)}, f32[2]{0:T(128)}, u32[]{:S(2)}) copy-start(f32[2]{0:T(128)} %param.23) | copy-start | bytes 28
  76.5 36.1 %all-to-all-start.1 = ((bf16[32,4,389]{2,1,0:T(4,128)(2,1)}), bf16[32,4,389]{2,1,0:T(4,128)(2,1)S(1)}, u32[]{:S(2)}, u32[]{:S(2)}) async-start(bf16[32,4,389]{2,1,0:T(4,128)(2,1)} %pad_maximum_fusion.1), calls=%async_computation.1 | async-start | bytes 262144 | tf_op jit(solution)/shard_map/all_to_all | solution.py:17
  85.3 17.7 %collective-permute-start.6 = (bf16[1,128,128]{2,1,0:T(8,128)(2,1)S(1)}, bf16[1,128,128]{2,1,0:T(8,128)(2,1)S(1)}, u32[]{:S(2)}, u32[]{:S(2)}) collective-permute-start(bf16[1,128,128]{2,1,0:T(8,128)(2,1)S(1)} %bitcast.98), channel_id=1, source_target_pairs={{0,48},{8,56},{16,32},{24,40},{32,16},{40,24},{48,0},{56,8},{1,49}... | collective-permute-start | bytes 98312 | tf_op jit(solution)/shard_map/ppermute | solution.py:62
  93.8 31.6 %collective-permute-start.7 = (bf16[1,128,128]{2,1,0:T(8,128)(2,1)S(1)}, bf16[1,128,128]{2,1,0:T(8,128)(2,1)S(1)}, u32[]{:S(2)}, u32[]{:S(2)}) collective-permute-start(bf16[1,128,128]{2,1,0:T(8,128)(2,1)S(1)} %bitcast.94), channel_id=1, source_target_pairs={{0,56},{8,48},{16,40},{24,32},{32,24},{40,16},{48,8},{56,0},{1,57}... | collective-permute-start | bytes 98312 | tf_op jit(solution)/shard_map/ppermute | solution.py:62
  103.1 11.2 %copy-start.1 = (f32[4,2,128,128]{3,2,1,0:T(8,128)S(1)}, f32[4,2,128,128]{3,2,1,0:T(8,128)}, u32[]{:S(2)}) copy-start(f32[4,2,128,128]{3,2,1,0:T(8,128)} %param.16) | copy-start | bytes 1572868
  113.3 0.7 copy-start.7
  115.0 0.7 copy-start.8
  116.4 31.8 %all-to-all-start.2 = ((bf16[32,4,256]{2,1,0:T(4,128)(2,1)}), bf16[32,4,256]{2,1,0:T(4,128)(2,1)S(1)}, u32[]{:S(2)}, u32[]{:S(2)}) async-start(bf16[32,4,256]{2,1,0:T(4,128)(2,1)} %broadcast_in_dim.15), calls=%async_computation.2 | async-start | bytes 131072 | tf_op jit(solution)/shard_map/all_to_all | solution.py:17
  219.6 17.3 %all-to-all-start.7 = ((bf16[8,8,128]{2,1,0:T(8,128)(2,1)}), bf16[8,8,128]{2,1,0:T(8,128)(2,1)S(1)}, u32[]{:S(2)}, u32[]{:S(2)}) async-start(bf16[8,8,128]{2,1,0:T(8,128)(2,1)} %bitcast.33), calls=%async_computation.7 | async-start | bytes 32768 | tf_op jit(solution)/shard_map/all_to_all | solution.py:17
where the time goes:
time: 239 us; the launch traced here: 238 us
  starting transfers between devices  103 us (43%)
  blocking collectives  69.9 us (29%)
  waiting for transfers between devices  46.6 us (19%)
  local copies, waits for them, and re-layouts  10.6 us (4%)
  other arithmetic  4.63 us (2%)
    all_to_all x4, starting transfers between devices, exchange(): return lax.all_to_all(x, axis, split_axis=0, concat_axis=0, tiled=True)  70.4 us
    all_to_all x4, blocking collectives, exchange(): return lax.all_to_all(x, axis, split_axis=0, concat_axis=0, tiled=True)  69.9 us
    all_to_all x4, waiting for transfers between devices, exchange(): return lax.all_to_all(x, axis, split_axis=0, concat_axis=0, tiled=True)  40.6 us
    ppermute x7, starting transfers between devices, mixer_weights(): piece = lax.ppermute(piece, LO, [(i, i ^ step) for i in range(near)])  29 us
    ppermute x7, waiting for transfers between devices, mixer_weights(): piece = lax.ppermute(piece, LO, [(i, i ^ step) for i in range(near)])  6.02 us
    unnamed x25, local copies, waits for them, and re-layouts  4.9 us
  transfers between devices with their start and end apart: 12, of which 4 were waited for; matrix products, arithmetic and copies ran while one was open for 4% of the time, Pallas kernels for 0%

commit v1 on v0

--- a/solution.py
+++ b/solution.py
@@ -10,7 +10,8 @@
 f32 = jnp.float32
 KV = ("hi", "mid", "pair")
 LO = ("mid", "pair")
-NEIGHBOURS = 8
+NEAR = (*LO, "tp")
+NEIGHBOURS = 4
 
 
 def exchange(x, axis):
@@ -47,7 +48,7 @@
     return (normed.astype(bf16), new_state)
 
 
-def mixer_weights(w_up, w_down, mixer_gain, n_tp):
+def mixer_weights(w_up, w_down, mixer_gain):
     near = lax.axis_size(LO)
     me = lax.axis_index(LO)
     block, wide = w_up.shape
@@ -62,8 +63,7 @@
             piece = lax.ppermute(piece, LO, [(i, i ^ step) for i in range(near)])
         whole = lax.dynamic_update_slice_in_dim(whole, piece, me ^ step, axis=0)
     up = whole[:, :block].reshape(near * block, share)
-    down_t = whole[:, block:].reshape(near, n_tp, block // n_tp, share)
-    down_t = down_t.transpose(1, 0, 2, 3).reshape(near * block, share)
+    down_t = whole[:, block:].reshape(near * block, share)
     return up, down_t
 
 
@@ -141,10 +141,9 @@
         dt_bias,
         head_gain,
     )
-    up, down_t = mixer_weights(w_up, w_down, mixer_gain, n_tp)
+    up, down_t = mixer_weights(w_up, w_down, mixer_gain)
 
     every = from_everyone(normed.reshape(seq_here, columns), KV).reshape(rows, columns)
-    every, up, down_t, new_state = lax.optimization_barrier((every, up, down_t, new_state))
     head_part = dotted(w_out, every, 0, 1).astype(bf16)
     attended = from_everyone(head_part, "tp").astype(f32).sum(axis=0)
     middle_block = (inputs + attended).astype(bf16)
@@ -154,15 +153,16 @@
     middle_f = middle.astype(f32)
     squares_two = jnp.sum(middle_f * middle_f, axis=0, keepdims=True)
     hidden_part = dotted(up, middle, 0, 0)
-    tail = jnp.broadcast_to(squares_two, (8, rows))
-    sent = jnp.concatenate([hidden_part, tail], axis=0).astype(bf16)
-    sums = from_everyone(sent, "hi").astype(f32).sum(axis=0)
+    far = lax.axis_size("hi")
+    hidden_part = hidden_part.reshape(far, -1, rows)
+    tail = jnp.broadcast_to(squares_two, (far, 8, rows))
+    sent = jnp.concatenate([hidden_part, tail], axis=1).astype(bf16)
+    sums = exchange(sent, "hi").astype(f32).sum(axis=0)
     second = lax.rsqrt(sums[-1:] / width + epsilon)
-    hidden = jnp.square(jax.nn.relu(second * sums[:-8])).astype(bf16)
+    hidden_own = jnp.square(jax.nn.relu(second * sums[:-8])).astype(bf16)
+    hidden = from_everyone(hidden_own, "hi").reshape(-1, rows)
     down_part = dotted(down_t, hidden, 1, 0).astype(bf16)
-    arrived = exchange(down_part.reshape(n_tp, n_near * own, rows), "tp")
-    near_part = arrived.astype(f32).sum(axis=0).astype(bf16)
-    arrived = exchange(near_part.reshape(n_near, own, rows), LO)
+    arrived = exchange(down_part.reshape(n_near * n_tp, own, rows), NEAR)
     lowered = arrived.astype(f32).sum(axis=0)
     mixed = (middle_own.astype(f32) + lowered).astype(bf16).T
     return (mixed, new_state)

time: 239 us -> 224 us (0.937)
  starting transfers between devices: 103 us -> 90.9 us
  blocking collectives: 69.9 us -> 58.1 us
  waiting for transfers between devices: 46.6 us -> 55.8 us
    ppermute x7 -> x3, starting transfers between devices: 29 us -> 9.36 us  [mixer_weights(): piece = lax.ppermute(piece, LO, [(i, i ^ step) for i in range(near)])]
    all_to_all x4 -> x6, waiting for transfers between devices: 40.6 us -> 55.8 us  [exchange(): return lax.all_to_all(x, axis, split_axis=0, concat_axis=0, tiled=True)]
    all_to_all x4 -> x2, blocking collectives: 69.9 us -> 58.1 us  [exchange(): return lax.all_to_all(x, axis, split_axis=0, concat_axis=0, tiled=True)]
    all_to_all x4 -> x6, starting transfers between devices: 70.4 us -> 78.1 us  [exchange(): return lax.all_to_all(x, axis, split_axis=0, concat_axis=0, tiled=True)]
    ppermute x7 -> x3, waiting for transfers between devices: 6.02 us -> 0.01 us  [mixer_weights(): piece = lax.ppermute(piece, LO, [(i, i ^ step) for i in range(near)])]
  transfers between devices with their start and end apart: 12 -> 10, of which waited for: 4 -> 5; matrix products, arithmetic and copies ran while one was open for 4% -> 3% of each run, Pallas kernels for 0% -> 0%
where the time goes in v1:
time: 224 us; the launch traced here: 223 us
  starting transfers between devices  90.9 us (41%)
  blocking collectives  58.1 us (26%)
  waiting for transfers between devices  55.8 us (25%)
  local copies, waits for them, and re-layouts  11.2 us (5%)
  other arithmetic  4.01 us (2%)
    all_to_all x6, starting transfers between devices, exchange(): return lax.all_to_all(x, axis, split_axis=0, concat_axis=0, tiled=True)  78.1 us
    all_to_all x2, blocking collectives, exchange(): return lax.all_to_all(x, axis, split_axis=0, concat_axis=0, tiled=True)  58.1 us
    all_to_all x6, waiting for transfers between devices, exchange(): return lax.all_to_all(x, axis, split_axis=0, concat_axis=0, tiled=True)  55.8 us
    ppermute x3, starting transfers between devices, mixer_weights(): piece = lax.ppermute(piece, LO, [(i, i ^ step) for i in range(near)])  9.36 us
    unnamed x25, local copies, waits for them, and re-layouts  4.64 us
  transfers between devices with their start and end apart: 10, of which 5 were waited for; matrix products, arithmetic and copies ran while one was open for 3% of the time, Pallas kernels for 0%

profile of v1, /device:TPU:33, one launch (start us, length us, event | category | flops | bytes accessed | tf_op | source)
XLA Modules:
  0.0 223.2 jit_solution(18103324300058553795)
XLA Ops:
  0.6 1.3 broadcast_in_dim.14
  2.0 44.9 %all-to-all-start = ((bf16[16,8,128]{2,1,0:T(8,128)(2,1)}), bf16[16,8,128]{2,1,0:T(8,128)(2,1)S(1)}, u32[]{:S(2)}, u32[]{:S(2)}) async-start(bf16[16,8,128]{2,1,0:T(8,128)(2,1)} %broadcast_in_dim.14), calls=%async_computation | async-start | bytes 65536 | tf_op jit(solution)/shard_map/all_to_all | solution.py:18
  46.8 0.6 copy-done.9
  47.5 0.7 copy-done.5
  48.3 0.7 copy-done.6
  49.0 0.1 multiply_convert_fusion.1
  49.2 0.2 constant_dynamic-slice_fusion.5
  49.4 3.4 %collective-permute-start = (bf16[64,384]{1,0:T(8,128)(2,1)S(1)}, bf16[64,384]{1,0:T(8,128)(2,1)S(1)}, u32[]{:S(2)}, u32[]{:S(2)}) collective-permute-start(bf16[64,384]{1,0:T(8,128)(2,1)S(1)} %bitcast.94), channel_id=1, source_target_pairs={{0,8},{8,0},{1,9},{9,1},{2,10},{10,2},{3,11},{11,3},{4,12},{12,4},... | collective-permute-start | bytes 147464 | tf_op jit(solution)/shard_map/ppermute | solution.py:107
  52.9 0.8 dynamic_slice.40
  53.6 0.8 dynamic_slice.39
  54.4 0.2 fusion.6
  54.6 0.2 convolution_convert_fusion.3
  54.8 0.2 convert_element_type.111
  55.1 0.1 copy.95
  55.2 0.2 fusion.1
  55.5 0.7 pad_maximum_fusion.1
  56.2 7.7 %all-to-all-start.1 = ((bf16[32,4,389]{2,1,0:T(4,128)(2,1)}), bf16[32,4,389]{2,1,0:T(4,128)(2,1)S(1)}, u32[]{:S(2)}, u32[]{:S(2)}) async-start(bf16[32,4,389]{2,1,0:T(4,128)(2,1)} %pad_maximum_fusion.1), calls=%async_computation.1 | async-start | bytes 262144 | tf_op jit(solution)/shard_map/all_to_all | solution.py:18
  63.9 28.7 %all-to-all-done.1 = bf16[32,4,389]{2,1,0:T(4,128)(2,1)S(1)} async-done(((bf16[32,4,389]{2,1,0:T(4,128)(2,1)}), bf16[32,4,389]{2,1,0:T(4,128)(2,1)S(1)}, u32[]{:S(2)}, u32[]{:S(2)}) %all-to-all-start.1) | async-done | bytes 99616 | tf_op jit(solution)/shard_map/all_to_all | solution.py:18
  92.6 0.2 rsqrt_reduce_fusion
  92.8 0.1 broadcast_multiply_fusion
  93.0 0.1 multiply_bitcast_fusion
  93.0 0.1 multiply_reduce_fusion.3
  93.1 0.1 fusion.56
  93.3 0.6 copy-done.7
  93.9 0.1 fusion.36
  94.0 0.1 copy.82
  94.1 0.1 copy.81
  94.2 0.1 fusion.32
  94.2 0.2 fusion.24
  94.4 0.2 fusion.26
  94.6 0.1 fusion.23
  94.7 0.2 multiply_reduce_fusion.1
  94.9 0.4 copy-done.8
  95.3 0.1 fusion.33
  95.4 0.7 broadcast_in_dim.15
  96.1 4.8 %all-to-all-start.2 = ((bf16[32,4,256]{2,1,0:T(4,128)(2,1)}), bf16[32,4,256]{2,1,0:T(4,128)(2,1)S(1)}, u32[]{:S(2)}, u32[]{:S(2)}) async-start(bf16[32,4,256]{2,1,0:T(4,128)(2,1)} %broadcast_in_dim.15), calls=%async_computation.2 | async-start | bytes 131072 | tf_op jit(solution)/shard_map/all_to_all | solution.py:18
  100.9 0.6 copy-done.11
  101.6 0.1 multiply_convert_fusion
  101.7 0.8 copy-done.3
  102.5 0.2 copy.83
  102.7 0.1 copy.85
  102.9 2.7 %collective-permute-start.1 = (bf16[1,128,256]{2,1,0:T(8,128)(2,1)S(1)}, bf16[1,128,256]{2,1,0:T(8,128)(2,1)S(1)}, u32[]{:S(2)}, u32[]{:S(2)}) collective-permute-start(bf16[1,128,256]{2,1,0:T(8,128)(2,1)S(1)} %bitcast.93), channel_id=1, source_target_pairs={{0,8},{8,0},{16,24},{24,16},{1,9},{9,1},{17,25},{25,17},{2,10},{10... | collective-permute-start | bytes 196616 | tf_op jit(solution)/shard_map/ppermute | solution.py:63
  105.6 0.1 copy.86
  105.7 4.0 %collective-permute-start.2 = (bf16[1,128,256]{2,1,0:T(8,128)(2,1)S(1)}, bf16[1,128,256]{2,1,0:T(8,128)(2,1)S(1)}, u32[]{:S(2)}, u32[]{:S(2)}) collective-permute-start(bf16[1,128,256]{2,1,0:T(8,128)(2,1)S(1)} %bitcast.92), channel_id=1, source_target_pairs={{0,16},{8,24},{16,0},{24,8},{1,17},{9,25},{17,1},{25,9},{2,18},{10... | collective-permute-start | bytes 196616 | tf_op jit(solution)/shard_map/ppermute | solution.py:63
  109.7 0.1 copy.87
  109.8 2.6 %collective-permute-start.3 = (bf16[1,128,256]{2,1,0:T(8,128)(2,1)S(1)}, bf16[1,128,256]{2,1,0:T(8,128)(2,1)S(1)}, u32[]{:S(2)}, u32[]{:S(2)}) collective-permute-start(bf16[1,128,256]{2,1,0:T(8,128)(2,1)S(1)} %bitcast.91), channel_id=1, source_target_pairs={{0,24},{8,16},{16,8},{24,0},{1,25},{9,17},{17,9},{25,1},{2,26},{10... | collective-permute-start | bytes 196616 | tf_op jit(solution)/shard_map/ppermute | solution.py:63
  112.5 0.1 copy.84
  112.6 11.1 %all-to-all-done.2 = bf16[32,4,256]{2,1,0:T(4,128)(2,1)S(1)} async-done(((bf16[32,4,256]{2,1,0:T(4,128)(2,1)}), bf16[32,4,256]{2,1,0:T(4,128)(2,1)S(1)}, u32[]{:S(2)}, u32[]{:S(2)}) %all-to-all-start.2) | async-done | bytes 65568 | tf_op jit(solution)/shard_map/all_to_all | solution.py:18
  123.7 0.1 fusion.3
  123.8 0.7 broadcast_in_dim.16
  124.5 8.4 %all-to-all-start.3 = ((bf16[8,64,128]{2,1,0:T(8,128)(2,1)}), bf16[8,64,128]{2,1,0:T(8,128)(2,1)S(1)}, u32[]{:S(2)}, u32[]{:S(2)}) async-start(bf16[8,64,128]{2,1,0:T(8,128)(2,1)} %broadcast_in_dim.16), calls=%async_computation.3 | async-start | bytes 262144 | tf_op jit(solution)/shard_map/all_to_all | solution.py:18
  133.0 5.2 %all-to-all-done.3 = bf16[8,64,128]{2,1,0:T(8,128)(2,1)S(1)} async-done(((bf16[8,64,128]{2,1,0:T(8,128)(2,1)}), bf16[8,64,128]{2,1,0:T(8,128)(2,1)S(1)}, u32[]{:S(2)}, u32[]{:S(2)}) %all-to-all-start.3) | async-done | bytes 131104 | tf_op jit(solution)/shard_map/all_to_all | solution.py:18
  138.2 0.6 broadcast_in_dim.18
  138.9 3.4 %all-to-all-start.4 = ((bf16[4,64,128]{2,1,0:T(8,128)(2,1)}), bf16[4,64,128]{2,1,0:T(8,128)(2,1)S(1)}, u32[]{:S(2)}, u32[]{:S(2)}) async-start(bf16[4,64,128]{2,1,0:T(8,128)(2,1)} %broadcast_in_dim.18), calls=%async_computation.4 | async-start | bytes 131072 | tf_op jit(solution)/shard_map/all_to_all | solution.py:18
  142.3 0.1 copy.88
  142.4 4.3 %all-to-all-done.4 = bf16[4,64,128]{2,1,0:T(8,128)(2,1)S(1)} async-done(((bf16[4,64,128]{2,1,0:T(8,128)(2,1)}), bf16[4,64,128]{2,1,0:T(8,128)(2,1)S(1)}, u32[]{:S(2)}, u32[]{:S(2)}) %all-to-all-start.4) | async-done | bytes 65568 | tf_op jit(solution)/shard_map/all_to_all | solution.py:18
  146.8 0.2 convolution_convert_fusion.1
  147.0 32.2 %all_to_all.40 = bf16[8,40,128]{2,1,0:T(8,128)(2,1)S(1)} all-to-all(bf16[8,40,128]{2,1,0:T(8,128)(2,1)S(1)} %pad_maximum_fusion.2), channel_id=1, replica_groups=mesh['grp'=2,'hi'=8,'mid'=2,'pair'=2,'tp'=8] {'hi'}, dimensions={0} | all-to-all | bytes 163840 | tf_op jit(solution)/shard_map/all_to_all | solution.py:18
  179.3 25.9 %all_to_all.41 = bf16[8,32,128]{2,1,0:T(8,128)(2,1)S(1)} all-to-all(bf16[8,32,128]{2,1,0:T(8,128)(2,1)S(1)} %broadcast_in_dim.20), channel_id=1, replica_groups=mesh['grp'=2,'hi'=8,'mid'=2,'pair'=2,'tp'=8] {'hi'}, dimensions={0} | all-to-all | bytes 131072 | tf_op jit(solution)/shard_map/all_to_all | solution.py:18
  205.2 0.8 fusion.2
  206.0 9.0 %all-to-all-start.7 = ((bf16[32,8,128]{2,1,0:T(8,128)(2,1)}), bf16[32,8,128]{2,1,0:T(8,128)(2,1)S(1)}, u32[]{:S(2)}, u32[]{:S(2)}) async-start(bf16[32,8,128]{2,1,0:T(8,128)(2,1)} %fusion.2), calls=%async_computation.7 | async-start | bytes 131072 | tf_op jit(solution)/shard_map/all_to_all | solution.py:18
  215.0 1.0 multiply_add_fusion
  216.0 6.6 %all-to-all-done.7 = bf16[32,8,128]{2,1,0:T(8,128)(2,1)S(1)} async-done(((bf16[32,8,128]{2,1,0:T(8,128)(2,1)}), bf16[32,8,128]{2,1,0:T(8,128)(2,1)S(1)}, u32[]{:S(2)}, u32[]{:S(2)}) %all-to-all-start.7) | async-done | bytes 65568 | tf_op jit(solution)/shard_map/all_to_all | solution.py:18
  222.6 0.6 fusion.34
  (59 shorter events, 0.7 us)
Async XLA Ops:
  0.6 123.1 %copy-start = (bf16[256,64]{0,1:T(8,128)(2,1)S(1)}, bf16[256,64]{0,1:T(8,128)(2,1)}, u32[]{:S(2)}) copy-start(bf16[256,64]{0,1:T(8,128)(2,1)} %param.26) | copy-start | bytes 98308
  2.0 45.5 %copy-start.4 = (bf16[64,256]{1,0:T(8,128)(2,1)S(1)}, bf16[64,256]{1,0:T(8,128)(2,1)}, u32[]{:S(2)}) copy-start(bf16[64,256]{1,0:T(8,128)(2,1)} %param.20) | copy-start | bytes 98308
  2.0 52.4 %all-to-all-start = ((bf16[16,8,128]{2,1,0:T(8,128)(2,1)}), bf16[16,8,128]{2,1,0:T(8,128)(2,1)S(1)}, u32[]{:S(2)}, u32[]{:S(2)}) async-start(bf16[16,8,128]{2,1,0:T(8,128)(2,1)} %broadcast_in_dim.14), calls=%async_computation | async-start | bytes 65536 | tf_op jit(solution)/shard_map/all_to_all | solution.py:18
  46.8 0.7 copy-start.9
  47.5 0.8 copy-start.5
  48.2 0.8 copy-start.6
  49.4 5.8 %collective-permute-start = (bf16[64,384]{1,0:T(8,128)(2,1)S(1)}, bf16[64,384]{1,0:T(8,128)(2,1)S(1)}, u32[]{:S(2)}, u32[]{:S(2)}) collective-permute-start(bf16[64,384]{1,0:T(8,128)(2,1)S(1)} %bitcast.94), channel_id=1, source_target_pairs={{0,8},{8,0},{1,9},{9,1},{2,10},{10,2},{3,11},{11,3},{4,12},{12,4},... | collective-permute-start | bytes 147464 | tf_op jit(solution)/shard_map/ppermute | solution.py:107
  56.2 7.7 %copy-start.10 = (f32[2]{0:T(128)S(1)}, f32[2]{0:T(128)}, u32[]{:S(2)}) copy-start(f32[2]{0:T(128)} %param.23) | copy-start | bytes 28
  56.2 36.3 %all-to-all-start.1 = ((bf16[32,4,389]{2,1,0:T(4,128)(2,1)}), bf16[32,4,389]{2,1,0:T(4,128)(2,1)S(1)}, u32[]{:S(2)}, u32[]{:S(2)}) async-start(bf16[32,4,389]{2,1,0:T(4,128)(2,1)} %pad_maximum_fusion.1), calls=%async_computation.1 | async-start | bytes 262144 | tf_op jit(solution)/shard_map/all_to_all | solution.py:18
  63.9 30.3 %copy-start.1 = (f32[4,2,128,128]{3,2,1,0:T(8,128)S(1)}, f32[4,2,128,128]{3,2,1,0:T(8,128)}, u32[]{:S(2)}) copy-start(f32[4,2,128,128]{3,2,1,0:T(8,128)} %param.16) | copy-start | bytes 1572868
  93.2 0.7 copy-start.7
  94.7 0.7 copy-start.8
  94.9 6.7 %copy-start.2 = (bf16[64,1024]{1,0:T(8,128)(2,1)S(1)}, bf16[64,1024]{1,0:T(8,128)(2,1)}, u32[]{:S(2)}) copy-start(bf16[64,1024]{1,0:T(8,128)(2,1)} %param.28) | copy-start | bytes 393220
  96.1 27.6 %all-to-all-start.2 = ((bf16[32,4,256]{2,1,0:T(4,128)(2,1)}), bf16[32,4,256]{2,1,0:T(4,128)(2,1)S(1)}, u32[]{:S(2)}, u32[]{:S(2)}) async-start(bf16[32,4,256]{2,1,0:T(4,128)(2,1)} %broadcast_in_dim.15), calls=%async_computation.2 | async-start | bytes 131072 | tf_op jit(solution)/shard_map/all_to_all | solution.py:18
  100.9 0.7 copy-start.11
  101.6 0.9 copy-start.3
  102.9 30.1 %collective-permute-start.1 = (bf16[1,128,256]{2,1,0:T(8,128)(2,1)S(1)}, bf16[1,128,256]{2,1,0:T(8,128)(2,1)S(1)}, u32[]{:S(2)}, u32[]{:S(2)}) collective-permute-start(bf16[1,128,256]{2,1,0:T(8,128)(2,1)S(1)} %bitcast.93), channel_id=1, source_target_pairs={{0,8},{8,0},{16,24},{24,16},{1,9},{9,1},{17,25},{25,17},{2,10},{10... | collective-permute-start | bytes 196616 | tf_op jit(solution)/shard_map/ppermute | solution.py:63
  105.7 36.6 %collective-permute-start.2 = (bf16[1,128,256]{2,1,0:T(8,128)(2,1)S(1)}, bf16[1,128,256]{2,1,0:T(8,128)(2,1)S(1)}, u32[]{:S(2)}, u32[]{:S(2)}) collective-permute-start(bf16[1,128,256]{2,1,0:T(8,128)(2,1)S(1)} %bitcast.92), channel_id=1, source_target_pairs={{0,16},{8,24},{16,0},{24,8},{1,17},{9,25},{17,1},{25,9},{2,18},{10... | collective-permute-start | bytes 196616 | tf_op jit(solution)/shard_map/ppermute | solution.py:63
  109.8 32.4 %collective-permute-start.3 = (bf16[1,128,256]{2,1,0:T(8,128)(2,1)S(1)}, bf16[1,128,256]{2,1,0:T(8,128)(2,1)S(1)}, u32[]{:S(2)}, u32[]{:S(2)}) collective-permute-start(bf16[1,128,256]{2,1,0:T(8,128)(2,1)S(1)} %bitcast.91), channel_id=1, source_target_pairs={{0,24},{8,16},{16,8},{24,0},{1,25},{9,17},{17,9},{25,1},{2,26},{10... | collective-permute-start | bytes 196616 | tf_op jit(solution)/shard_map/ppermute | solution.py:63
  124.5 13.6 %all-to-all-start.3 = ((bf16[8,64,128]{2,1,0:T(8,128)(2,1)}), bf16[8,64,128]{2,1,0:T(8,128)(2,1)S(1)}, u32[]{:S(2)}, u32[]{:S(2)}) async-start(bf16[8,64,128]{2,1,0:T(8,128)(2,1)} %broadcast_in_dim.16), calls=%async_computation.3 | async-start | bytes 262144 | tf_op jit(solution)/shard_map/all_to_all | solution.py:18
  138.9 7.9 %all-to-all-start.4 = ((bf16[4,64,128]{2,1,0:T(8,128)(2,1)}), bf16[4,64,128]{2,1,0:T(8,128)(2,1)S(1)}, u32[]{:S(2)}, u32[]{:S(2)}) async-start(bf16[4,64,128]{2,1,0:T(8,128)(2,1)} %broadcast_in_dim.18), calls=%async_computation.4 | async-start | bytes 131072 | tf_op jit(solution)/shard_map/all_to_all | solution.py:18
  206.0 16.6 %all-to-all-start.7 = ((bf16[32,8,128]{2,1,0:T(8,128)(2,1)}), bf16[32,8,128]{2,1,0:T(8,128)(2,1)S(1)}, u32[]{:S(2)}, u32[]{:S(2)}) async-start(bf16[32,8,128]{2,1,0:T(8,128)(2,1)} %fusion.2), calls=%async_computation.7 | async-start | bytes 131072 | tf_op jit(solution)/shard_map/all_to_all | solution.py:18

commit v2 on v1

--- a/solution.py
+++ b/solution.py
@@ -48,20 +48,26 @@
     return (normed.astype(bf16), new_state)
 
 
-def mixer_weights(w_up, w_down, mixer_gain):
+def mixer_pieces(w_up, w_down, mixer_gain):
     near = lax.axis_size(LO)
     me = lax.axis_index(LO)
     block, wide = w_up.shape
-    share = wide // near
     gained = (w_up.astype(f32) * mixer_gain.astype(f32)[:, None]).astype(bf16)
     both = jnp.concatenate([gained, w_down.T], axis=0)
-    both = both.reshape(2 * block, near, share).transpose(1, 0, 2)
-    whole = jnp.zeros_like(both)
-    for step in range(near):
-        piece = lax.dynamic_slice_in_dim(both, me ^ step, 1, axis=0)
+    both = both.reshape(2 * block, near, wide // near).transpose(1, 0, 2)
+    return [lax.dynamic_index_in_dim(both, me ^ step, 0, keepdims=False) for step in range(near)]
+
+
+def mixer_weights(pieces):
+    near = lax.axis_size(LO)
+    me = lax.axis_index(LO)
+    both, share = pieces[0].shape
+    whole = jnp.zeros((near, both, share), bf16)
+    for step, piece in enumerate(pieces):
         if step:
             piece = lax.ppermute(piece, LO, [(i, i ^ step) for i in range(near)])
-        whole = lax.dynamic_update_slice_in_dim(whole, piece, me ^ step, axis=0)
+        whole = lax.dynamic_update_slice_in_dim(whole, piece[None], me ^ step, axis=0)
+    block = both // 2
     up = whole[:, :block].reshape(near * block, share)
     down_t = whole[:, block:].reshape(near * block, share)
     return up, down_t
@@ -121,7 +127,9 @@
         squares[:, None].astype(bf16),
     ]
     sent = jnp.concatenate(parts, axis=1).reshape(n_kv, seq_here, -1)
+    pieces = mixer_pieces(w_up, w_down, mixer_gain)
     arrived = exchange(sent, KV)
+    arrived, *pieces = lax.optimization_barrier((arrived, *pieces))
     main = 3 * head_size
     sums = arrived.astype(f32)
     gates = sums[..., main:].sum(axis=0)
@@ -141,7 +149,7 @@
         dt_bias,
         head_gain,
     )
-    up, down_t = mixer_weights(w_up, w_down, mixer_gain)
+    up, down_t = mixer_weights(pieces)
 
     every = from_everyone(normed.reshape(seq_here, columns), KV).reshape(rows, columns)
     head_part = dotted(w_out, every, 0, 1).astype(bf16)

time: 224 us -> 222 us (level)
  blocking collectives: 58.1 us -> 55.8 us
    all_to_all x2, blocking collectives: 58.1 us -> 55.8 us  [exchange(): return lax.all_to_all(x, axis, split_axis=0, concat_axis=0, tiled=True)]
where the time goes in v2:
time: 222 us; the launch traced here: 221 us
  starting transfers between devices  91.1 us (41%)
  blocking collectives  55.8 us (25%)
  waiting for transfers between devices  55.3 us (25%)
  local copies, waits for them, and re-layouts  12 us (5%)
  other arithmetic  4.01 us (2%)
    all_to_all x6, starting transfers between devices, exchange(): return lax.all_to_all(x, axis, split_axis=0, concat_axis=0, tiled=True)  78.3 us
    all_to_all x2, blocking collectives, exchange(): return lax.all_to_all(x, axis, split_axis=0, concat_axis=0, tiled=True)  55.8 us
    all_to_all x6, waiting for transfers between devices, exchange(): return lax.all_to_all(x, axis, split_axis=0, concat_axis=0, tiled=True)  55.3 us
    ppermute x3, starting transfers between devices, mixer_weights(): piece = lax.ppermute(piece, LO, [(i, i ^ step) for i in range(near)])  9.36 us
    unnamed x25, local copies, waits for them, and re-layouts  5.43 us
  transfers between devices with their start and end apart: 10, of which 5 were waited for; matrix products, arithmetic and copies ran while one was open for 3% of the time, Pallas kernels for 0%

profile of v2, /device:TPU:33, one launch (start us, length us, event | category | flops | bytes accessed | tf_op | source)
XLA Modules:
  0.0 221.3 jit_solution(15801238649241070967)
XLA Ops:
  0.6 1.3 broadcast_in_dim.22
  2.0 44.9 %all-to-all-start = ((bf16[16,8,128]{2,1,0:T(8,128)(2,1)}), bf16[16,8,128]{2,1,0:T(8,128)(2,1)S(1)}, u32[]{:S(2)}, u32[]{:S(2)}) async-start(bf16[16,8,128]{2,1,0:T(8,128)(2,1)} %broadcast_in_dim.22), calls=%async_computation | async-start | bytes 65536 | tf_op jit(solution)/shard_map/all_to_all | solution.py:18
  46.8 0.6 copy-done.9
  47.5 0.7 copy-done.5
  48.3 0.7 copy-done.6
  49.0 0.1 multiply_convert_fusion.1
  49.2 0.2 constant_dynamic-slice_fusion.5
  49.4 3.4 %collective-permute-start = (bf16[64,384]{1,0:T(8,128)(2,1)S(1)}, bf16[64,384]{1,0:T(8,128)(2,1)S(1)}, u32[]{:S(2)}, u32[]{:S(2)}) collective-permute-start(bf16[64,384]{1,0:T(8,128)(2,1)S(1)} %bitcast.102), channel_id=1, source_target_pairs={{0,8},{8,0},{1,9},{9,1},{2,10},{10,2},{3,11},{11,3},{4,12},{12,4},... | collective-permute-start | bytes 147464 | tf_op jit(solution)/shard_map/ppermute | solution.py:113
  52.9 0.8 dynamic_slice.32
  53.6 0.8 dynamic_slice.33
  54.4 0.2 fusion.6
  54.6 0.2 convolution_convert_fusion.3
  54.8 0.1 copy.95
  55.0 0.2 convert_element_type.111
  55.2 0.2 fusion.1
  55.5 0.7 pad_maximum_fusion.1
  56.2 7.7 %all-to-all-start.1 = ((bf16[32,4,389]{2,1,0:T(4,128)(2,1)}), bf16[32,4,389]{2,1,0:T(4,128)(2,1)S(1)}, u32[]{:S(2)}, u32[]{:S(2)}) async-start(bf16[32,4,389]{2,1,0:T(4,128)(2,1)} %pad_maximum_fusion.1), calls=%async_computation.1 | async-start | bytes 262144 | tf_op jit(solution)/shard_map/all_to_all | solution.py:18
  63.9 0.6 copy-done.10
  64.6 0.1 multiply_convert_fusion
  64.7 0.8 copy-done.3
  65.5 0.2 copy.81
  65.7 0.1 copy.85
  65.8 0.1 copy.84
  65.9 0.1 copy.83
  66.1 0.1 copy.82
  66.2 0.5 copy-done.11
  66.7 25.8 %all-to-all-done.1 = bf16[32,4,389]{2,1,0:T(4,128)(2,1)S(1)} async-done(((bf16[32,4,389]{2,1,0:T(4,128)(2,1)}), bf16[32,4,389]{2,1,0:T(4,128)(2,1)S(1)}, u32[]{:S(2)}, u32[]{:S(2)}) %all-to-all-start.1) | async-done | bytes 99616 | tf_op jit(solution)/shard_map/all_to_all | solution.py:18
  92.7 0.2 rsqrt_reduce_fusion
  92.9 0.1 broadcast_multiply_fusion
  93.1 0.1 multiply_reduce_fusion.3
  93.2 0.1 slice_multiply_fusion.1
  93.3 0.6 copy-done.7
  93.9 0.1 fusion.36
  94.0 0.1 copy.87
  94.1 0.1 copy.86
  94.2 0.1 fusion.32
  94.2 0.2 fusion.26
  94.4 0.2 fusion.24
  94.6 0.1 fusion.23
  94.7 0.2 multiply_reduce_fusion.1
  94.9 0.7 copy-done.8
  95.6 0.1 fusion.33
  95.7 0.7 broadcast_in_dim.23
  96.3 4.8 %all-to-all-start.2 = ((bf16[32,4,256]{2,1,0:T(4,128)(2,1)}), bf16[32,4,256]{2,1,0:T(4,128)(2,1)S(1)}, u32[]{:S(2)}, u32[]{:S(2)}) async-start(bf16[32,4,256]{2,1,0:T(4,128)(2,1)} %broadcast_in_dim.23), calls=%async_computation.2 | async-start | bytes 131072 | tf_op jit(solution)/shard_map/all_to_all | solution.py:18
  101.2 2.7 %collective-permute-start.1 = (bf16[128,256]{1,0:T(8,128)(2,1)S(1)}, bf16[128,256]{1,0:T(8,128)(2,1)S(1)}, u32[]{:S(2)}, u32[]{:S(2)}) collective-permute-start(bf16[128,256]{1,0:T(8,128)(2,1)S(1)} %bitcast.101), channel_id=1, source_target_pairs={{0,8},{8,0},{16,24},{24,16},{1,9},{9,1},{17,25},{25,17},{2,10},{10... | collective-permute-start | bytes 196616 | tf_op jit(solution)/shard_map/ppermute | solution.py:68
  103.9 4.0 %collective-permute-start.2 = (bf16[128,256]{1,0:T(8,128)(2,1)S(1)}, bf16[128,256]{1,0:T(8,128)(2,1)S(1)}, u32[]{:S(2)}, u32[]{:S(2)}) collective-permute-start(bf16[128,256]{1,0:T(8,128)(2,1)S(1)} %bitcast.100), channel_id=1, source_target_pairs={{0,16},{8,24},{16,0},{24,8},{1,17},{9,25},{17,1},{25,9},{2,18},{10... | collective-permute-start | bytes 196616 | tf_op jit(solution)/shard_map/ppermute | solution.py:68
  107.9 2.6 %collective-permute-start.3 = (bf16[128,256]{1,0:T(8,128)(2,1)S(1)}, bf16[128,256]{1,0:T(8,128)(2,1)S(1)}, u32[]{:S(2)}, u32[]{:S(2)}) collective-permute-start(bf16[128,256]{1,0:T(8,128)(2,1)S(1)} %bitcast.99), channel_id=1, source_target_pairs={{0,24},{8,16},{16,8},{24,0},{1,25},{9,17},{17,9},{25,1},{2,26},{10... | collective-permute-start | bytes 196616 | tf_op jit(solution)/shard_map/ppermute | solution.py:68
  110.6 13.3 %all-to-all-done.2 = bf16[32,4,256]{2,1,0:T(4,128)(2,1)S(1)} async-done(((bf16[32,4,256]{2,1,0:T(4,128)(2,1)}), bf16[32,4,256]{2,1,0:T(4,128)(2,1)S(1)}, u32[]{:S(2)}, u32[]{:S(2)}) %all-to-all-start.2) | async-done | bytes 65568 | tf_op jit(solution)/shard_map/all_to_all | solution.py:18
  123.9 0.1 fusion.3
  124.0 0.7 broadcast_in_dim.24
  124.8 8.6 %all-to-all-start.3 = ((bf16[8,64,128]{2,1,0:T(8,128)(2,1)}), bf16[8,64,128]{2,1,0:T(8,128)(2,1)S(1)}, u32[]{:S(2)}, u32[]{:S(2)}) async-start(bf16[8,64,128]{2,1,0:T(8,128)(2,1)} %broadcast_in_dim.24), calls=%async_computation.3 | async-start | bytes 262144 | tf_op jit(solution)/shard_map/all_to_all | solution.py:18
  133.3 5.2 %all-to-all-done.3 = bf16[8,64,128]{2,1,0:T(8,128)(2,1)S(1)} async-done(((bf16[8,64,128]{2,1,0:T(8,128)(2,1)}), bf16[8,64,128]{2,1,0:T(8,128)(2,1)S(1)}, u32[]{:S(2)}, u32[]{:S(2)}) %all-to-all-start.3) | async-done | bytes 131104 | tf_op jit(solution)/shard_map/all_to_all | solution.py:18
  138.6 0.6 broadcast_in_dim.30
  139.2 3.4 %all-to-all-start.4 = ((bf16[4,64,128]{2,1,0:T(8,128)(2,1)}), bf16[4,64,128]{2,1,0:T(8,128)(2,1)S(1)}, u32[]{:S(2)}, u32[]{:S(2)}) async-start(bf16[4,64,128]{2,1,0:T(8,128)(2,1)} %broadcast_in_dim.30), calls=%async_computation.4 | async-start | bytes 131072 | tf_op jit(solution)/shard_map/all_to_all | solution.py:18
  142.7 0.1 copy.88
  142.8 4.4 %all-to-all-done.4 = bf16[4,64,128]{2,1,0:T(8,128)(2,1)S(1)} async-done(((bf16[4,64,128]{2,1,0:T(8,128)(2,1)}), bf16[4,64,128]{2,1,0:T(8,128)(2,1)S(1)}, u32[]{:S(2)}, u32[]{:S(2)}) %all-to-all-start.4) | async-done | bytes 65568 | tf_op jit(solution)/shard_map/all_to_all | solution.py:18
  147.1 0.2 convolution_convert_fusion.1
  147.4 29.9 %all_to_all.40 = bf16[8,40,128]{2,1,0:T(8,128)(2,1)S(1)} all-to-all(bf16[8,40,128]{2,1,0:T(8,128)(2,1)S(1)} %pad_maximum_fusion.2), channel_id=1, replica_groups=mesh['grp'=2,'hi'=8,'mid'=2,'pair'=2,'tp'=8] {'hi'}, dimensions={0} | all-to-all | bytes 163840 | tf_op jit(solution)/shard_map/all_to_all | solution.py:18
  177.3 25.9 %all_to_all.41 = bf16[8,32,128]{2,1,0:T(8,128)(2,1)S(1)} all-to-all(bf16[8,32,128]{2,1,0:T(8,128)(2,1)S(1)} %broadcast_in_dim.63), channel_id=1, replica_groups=mesh['grp'=2,'hi'=8,'mid'=2,'pair'=2,'tp'=8] {'hi'}, dimensions={0} | all-to-all | bytes 131072 | tf_op jit(solution)/shard_map/all_to_all | solution.py:18
  203.2 0.8 fusion.2
  204.0 9.0 %all-to-all-start.7 = ((bf16[32,8,128]{2,1,0:T(8,128)(2,1)}), bf16[32,8,128]{2,1,0:T(8,128)(2,1)S(1)}, u32[]{:S(2)}, u32[]{:S(2)}) async-start(bf16[32,8,128]{2,1,0:T(8,128)(2,1)} %fusion.2), calls=%async_computation.7 | async-start | bytes 131072 | tf_op jit(solution)/shard_map/all_to_all | solution.py:18
  213.0 1.0 multiply_add_fusion
  214.0 6.6 %all-to-all-done.7 = bf16[32,8,128]{2,1,0:T(8,128)(2,1)S(1)} async-done(((bf16[32,8,128]{2,1,0:T(8,128)(2,1)}), bf16[32,8,128]{2,1,0:T(8,128)(2,1)S(1)}, u32[]{:S(2)}, u32[]{:S(2)}) %all-to-all-start.7) | async-done | bytes 65568 | tf_op jit(solution)/shard_map/all_to_all | solution.py:18
  220.7 0.6 fusion.34
  (59 shorter events, 0.8 us)
Async XLA Ops:
  0.6 123.3 %copy-start = (bf16[256,64]{0,1:T(8,128)(2,1)S(1)}, bf16[256,64]{0,1:T(8,128)(2,1)}, u32[]{:S(2)}) copy-start(bf16[256,64]{0,1:T(8,128)(2,1)} %param.26) | copy-start | bytes 98308
  2.0 45.5 %copy-start.4 = (bf16[64,256]{1,0:T(8,128)(2,1)S(1)}, bf16[64,256]{1,0:T(8,128)(2,1)}, u32[]{:S(2)}) copy-start(bf16[64,256]{1,0:T(8,128)(2,1)} %param.18) | copy-start | bytes 98308
  2.0 52.4 %all-to-all-start = ((bf16[16,8,128]{2,1,0:T(8,128)(2,1)}), bf16[16,8,128]{2,1,0:T(8,128)(2,1)S(1)}, u32[]{:S(2)}, u32[]{:S(2)}) async-start(bf16[16,8,128]{2,1,0:T(8,128)(2,1)} %broadcast_in_dim.22), calls=%async_computation | async-start | bytes 65536 | tf_op jit(solution)/shard_map/all_to_all | solution.py:18
  46.8 0.7 copy-start.9
  47.5 0.8 copy-start.5
  48.2 0.8 copy-start.6
  49.4 5.8 %collective-permute-start = (bf16[64,384]{1,0:T(8,128)(2,1)S(1)}, bf16[64,384]{1,0:T(8,128)(2,1)S(1)}, u32[]{:S(2)}, u32[]{:S(2)}) collective-permute-start(bf16[64,384]{1,0:T(8,128)(2,1)S(1)} %bitcast.102), channel_id=1, source_target_pairs={{0,8},{8,0},{1,9},{9,1},{2,10},{10,2},{3,11},{11,3},{4,12},{12,4},... | collective-permute-start | bytes 147464 | tf_op jit(solution)/shard_map/ppermute | solution.py:113
  56.2 8.3 %copy-start.2 = (bf16[64,1024]{1,0:T(8,128)(2,1)S(1)}, bf16[64,1024]{1,0:T(8,128)(2,1)}, u32[]{:S(2)}) copy-start(bf16[64,1024]{1,0:T(8,128)(2,1)} %param.28) | copy-start | bytes 393220
  56.2 36.3 %all-to-all-start.1 = ((bf16[32,4,389]{2,1,0:T(4,128)(2,1)}), bf16[32,4,389]{2,1,0:T(4,128)(2,1)S(1)}, u32[]{:S(2)}, u32[]{:S(2)}) async-start(bf16[32,4,389]{2,1,0:T(4,128)(2,1)} %pad_maximum_fusion.1), calls=%async_computation.1 | async-start | bytes 262144 | tf_op jit(solution)/shard_map/all_to_all | solution.py:18
  63.9 0.7 copy-start.10
  64.6 0.9 copy-start.3
  66.1 0.7 copy-start.11
  92.6 1.7 copy-start.1
  93.2 0.7 copy-start.7
  94.9 0.7 copy-start.8
  96.3 27.6 %all-to-all-start.2 = ((bf16[32,4,256]{2,1,0:T(4,128)(2,1)}), bf16[32,4,256]{2,1,0:T(4,128)(2,1)S(1)}, u32[]{:S(2)}, u32[]{:S(2)}) async-start(bf16[32,4,256]{2,1,0:T(4,128)(2,1)} %broadcast_in_dim.23), calls=%async_computation.2 | async-start | bytes 131072 | tf_op jit(solution)/shard_map/all_to_all | solution.py:18
  101.2 9.4 %collective-permute-start.1 = (bf16[128,256]{1,0:T(8,128)(2,1)S(1)}, bf16[128,256]{1,0:T(8,128)(2,1)S(1)}, u32[]{:S(2)}, u32[]{:S(2)}) collective-permute-start(bf16[128,256]{1,0:T(8,128)(2,1)S(1)} %bitcast.101), channel_id=1, source_target_pairs={{0,8},{8,0},{16,24},{24,16},{1,9},{9,1},{17,25},{25,17},{2,10},{10... | collective-permute-start | bytes 196616 | tf_op jit(solution)/shard_map/ppermute | solution.py:68
  103.9 29.4 %collective-permute-start.2 = (bf16[128,256]{1,0:T(8,128)(2,1)S(1)}, bf16[128,256]{1,0:T(8,128)(2,1)S(1)}, u32[]{:S(2)}, u32[]{:S(2)}) collective-permute-start(bf16[128,256]{1,0:T(8,128)(2,1)S(1)} %bitcast.100), channel_id=1, source_target_pairs={{0,16},{8,24},{16,0},{24,8},{1,17},{9,25},{17,1},{25,9},{2,18},{10... | collective-permute-start | bytes 196616 | tf_op jit(solution)/shard_map/ppermute | solution.py:68
  107.9 34.7 %collective-permute-start.3 = (bf16[128,256]{1,0:T(8,128)(2,1)S(1)}, bf16[128,256]{1,0:T(8,128)(2,1)S(1)}, u32[]{:S(2)}, u32[]{:S(2)}) collective-permute-start(bf16[128,256]{1,0:T(8,128)(2,1)S(1)} %bitcast.99), channel_id=1, source_target_pairs={{0,24},{8,16},{16,8},{24,0},{1,25},{9,17},{17,9},{25,1},{2,26},{10... | collective-permute-start | bytes 196616 | tf_op jit(solution)/shard_map/ppermute | solution.py:68
  124.8 13.8 %all-to-all-start.3 = ((bf16[8,64,128]{2,1,0:T(8,128)(2,1)}), bf16[8,64,128]{2,1,0:T(8,128)(2,1)S(1)}, u32[]{:S(2)}, u32[]{:S(2)}) async-start(bf16[8,64,128]{2,1,0:T(8,128)(2,1)} %broadcast_in_dim.24), calls=%async_computation.3 | async-start | bytes 262144 | tf_op jit(solution)/shard_map/all_to_all | solution.py:18
  139.2 7.9 %all-to-all-start.4 = ((bf16[4,64,128]{2,1,0:T(8,128)(2,1)}), bf16[4,64,128]{2,1,0:T(8,128)(2,1)S(1)}, u32[]{:S(2)}, u32[]{:S(2)}) async-start(bf16[4,64,128]{2,1,0:T(8,128)(2,1)} %broadcast_in_dim.30), calls=%async_computation.4 | async-start | bytes 131072 | tf_op jit(solution)/shard_map/all_to_all | solution.py:18
  204.0 16.6 %all-to-all-start.7 = ((bf16[32,8,128]{2,1,0:T(8,128)(2,1)}), bf16[32,8,128]{2,1,0:T(8,128)(2,1)S(1)}, u32[]{:S(2)}, u32[]{:S(2)}) async-start(bf16[32,8,128]{2,1,0:T(8,128)(2,1)} %fusion.2), calls=%async_computation.7 | async-start | bytes 131072 | tf_op jit(solution)/shard_map/all_to_all | solution.py:18
